TPU v7x, 32 devices: a whole 2x2x4 slice. The times are simulated.
32 devices in a mesh: sp: 4 (over z), fs: 4 (over y, core), tp: 2 (over x).
Axes of the slice: x: 2, y: 2, z: 4, core: 2. Of those that a mesh axis runs over, the one named last changes fastest.
Arguments:
- tokens: bfloat16 [4096, 2048], P(('fs', 'sp', 'tp')), parts along dimension 0, may hold values from -6 to 6
- norm_gain: bfloat16 [2048], replicated, may hold values from 0.099609375 to 1.8984375
- w_pool_in: bfloat16 [2048, 1024], P('sp', 'tp'), may hold values from -0.125 to 0.125
- w_query: bfloat16 [2048, 1024], P('sp', 'tp'), may hold values from -0.125 to 0.125
- w_key: bfloat16 [2048, 1024], P('sp', 'tp'), may hold values from -0.125 to 0.125
- w_value: bfloat16 [2048, 1024], P('sp', 'tp'), may hold values from -0.125 to 0.125
- w_gate: bfloat16 [2048, 1024], P('sp', 'tp'), may hold values from -0.125 to 0.125
- w_beta: bfloat16 [2048, 8], replicated, may hold values from -0.125 to 0.125
- w_decay: bfloat16 [2048, 8], replicated, may hold values from -0.5 to 0.5
- conv_weight: float32 [3, 4, 1024], P(None, None, 'tp'), may hold values from -3 to 3
- a_log: float32 [8], P('tp'), may hold values from -20 to -1.7, as said below
- decay_extra: float32 [4096, 8], P(('fs', 'sp'), 'tp'), parts along dimension 0, may hold values from -1.4 to 0
- w_mix: bfloat16 [8, 128, 128], P('tp'), may hold values from -0.5 to 0.5
- pool_scale: float32 [1024], P('tp'), may hold values from 0.1 to 1.9
- delta_gain: float32 [128], replicated, may hold values from 0.1 to 1.9
- w_out_pool: bfloat16 [1024, 2048], P('tp', 'sp'), may hold values from -0.125 to 0.125
- w_out_delta: bfloat16 [1024, 2048], P('tp', 'sp'), may hold values from -0.125 to 0.125
Outputs:
- mixed: bfloat16 [4096, 2048], P(('fs', 'sp', 'tp')), parts along dimension 0
There are 4 independent parts, one for each index of `fs`. A program takes and returns all parts, laid end to end along the dimension named above; an argument that names none is the same for every part. Nothing has to cross between parts.
Inputs may be any that keep to these rules, and one draw needn't show every extreme that they name: `a_log`: logarithm of each head's base decay rate.
All inputs are finite; a program needn't handle non-finite values.
Results may differ from a plain program's by a relative error of at most 0.018.
Values may be sent and summed in bfloat16 or wider, within the bound.
A program may use at most 64 MiB of HBM per device.

v0:
```python
import functools

import jax
import jax.numpy as jnp
from jax import lax
from jax.experimental import pallas as pl
from jax.experimental.pallas import tpu as pltpu
from jax.sharding import PartitionSpec as P

BLOCK = 64
PAIR = 2 * BLOCK

eps = 1e-06
halo = 16
MESH = pl.DeviceIdType.MESH
highest = lax.Precision.HIGHEST
f32 = jnp.float32
bf16 = jnp.bfloat16
KEY, QUERY, VALUE, POOL, GATE, OUT_POOL, OUT_DELTA = range(7)
AHEAD = 1


def mm(a, b, dims=((1,), (0,)), precision=highest):
    return lax.dot_general(a, b, (dims, ((), ())), precision=precision, preferred_element_type=f32)


def rms_rows(values, gain):
    floats = values.astype(f32)
    scale = lax.rsqrt(jnp.mean(floats * floats, axis=-1, keepdims=True) + eps)
    return (floats * scale * gain.astype(f32)).astype(bf16)


def unit_rows(values):
    return values * lax.rsqrt(jnp.sum(values * values, axis=-1, keepdims=True) + eps)


def silu(x):
    return x * jax.nn.sigmoid(x)


def share_bits(n_fs):
    if n_fs & (n_fs - 1):
        return []
    return [n_fs >> (k + 1) for k in range(n_fs.bit_length() - 1)]


class Gather:
    def __init__(self, n_sp, n_fs, wbuf, z_s, z_r, f_s, f_r):
        self.n_sp, self.bits = n_sp, share_bits(n_fs)
        self.wbuf, self.z_s, self.z_r, self.f_s, self.f_r = wbuf, z_s, z_r, f_s, f_r
        self.sp, self.fs = lax.axis_index("sp"), lax.axis_index("fs")
        self.pieces = 2 ** len(self.bits)
        self.mine = self.fs if self.bits else 0 * self.fs
        self.depth = wbuf.shape[2] // self.pieces

    def partner(self, bit):
        return self.fs + bit * (1 - 2 * (self.fs // bit % 2))

    def mask_of(self, m, index):
        for i, bit in enumerate(self.bits):
            if m >> i & 1:
                index = index + bit * (1 - 2 * (index // bit % 2))
        return index

    def piece(self, w, src, index):
        return self.wbuf.at[w, src, pl.ds(pl.multiple_of(index * self.depth, self.depth), self.depth)]

    def z_copy(self, w, src, way):
        ref = self.piece(w, src, self.mine)
        to = lax.rem(self.sp + way + self.n_sp, self.n_sp)
        return pltpu.make_async_remote_copy(
            src_ref=ref, dst_ref=ref, send_sem=self.z_s.at[w, src, (way + 1) // 2], recv_sem=self.z_r.at[w, src],
            device_id={"sp": to}, device_id_type=MESH)

    def f_copy(self, w, src, k, m):
        slot = 2 ** k - 1 + m
        ref = self.piece(w, src, self.mask_of(m, self.mine))
        return pltpu.make_async_remote_copy(
            src_ref=ref, dst_ref=ref, send_sem=self.f_s.at[w, src, slot], recv_sem=self.f_r.at[w, src, slot],
            device_id={"fs": self.partner(self.bits[k])}, device_id_type=MESH)

    def can_send(self, way):
        return self.sp < self.n_sp - 1 if way == 1 else self.sp > 0

    def send(self, w):
        for way in (1, -1):
            @pl.when(self.can_send(way))
            def _():
                self.z_copy(w, self.sp, way).start()

    def each(self, t, act):
        for way in (1, -1):
            src = self.sp - way * t
            @pl.when(src >= 0 if way == 1 else src < self.n_sp)
            def _():
                act(src, way)

    def arrive_z(self, w, src, way):
        self.z_copy(w, src, way).wait_recv()

        @pl.when(self.can_send(way))
        def _():
            self.z_copy(w, src, way).start()
        for k in range(len(self.bits)):
            self.f_copy(w, src, k, 0).start()

    def arrive_f(self, w, t, k):
        def act(src, way):
            for m in range(2 ** k):
                self.f_copy(w, src, k, m).wait_recv()
                for later in range(k + 1, len(self.bits)):
                    self.f_copy(w, src, later, m | 1 << k).start()
        self.each(t, act)

    def forward(self, w):
        last = self.n_sp - 1
        inner = len(self.bits) - 1
        if w + AHEAD < self.wbuf.shape[0]:
            self.send(w + AHEAD)

        def body(t, c):
            self.each(t, lambda src, way: self.arrive_z(w, src, way))
            for k in range(inner):
                @pl.when(t > 1)
                def _():
                    self.arrive_f(w, t - 1, k)
                if w > 0:
                    @pl.when(t == 1)
                    def _():
                        self.arrive_f(w - 1, last, k)
            return c
        lax.fori_loop(1, self.n_sp, body, 0)

    def flush(self, w):
        for k in range(len(self.bits) - 1):
            self.arrive_f(w, self.n_sp - 1, k)

    def finish(self, w):
        if self.bits:
            def body(t, c):
                self.arrive_f(w, t, len(self.bits) - 1)
                return c
            lax.fori_loop(1, self.n_sp, body, 0)

    def drain(self, w):
        for way in (1, -1):
            @pl.when(self.can_send(way))
            def _():
                self.z_copy(w, self.sp, way).wait_send()

        def act(src, way):
            @pl.when(self.can_send(way))
            def _():
                self.z_copy(w, src, way).wait_send()
            for k in range(len(self.bits)):
                for m in range(2 ** k):
                    self.f_copy(w, src, k, m).wait_send()

        def body(t, c):
            self.each(t, act)
            return c
        lax.fori_loop(1, self.n_sp, body, 0)


def enter(n_sp, n_fs, n_tp):
    sp, fs, tp = (lax.axis_index(a) for a in ("sp", "fs", "tp"))
    barrier = pltpu.get_barrier_semaphore()
    bits = share_bits(n_fs)
    for d in range(1, n_sp):
        pl.semaphore_signal(barrier, inc=1, device_id={"sp": lax.rem(sp + d, n_sp)}, device_id_type=MESH)
    for bit in bits:
        pl.semaphore_signal(barrier, inc=1, device_id={"fs": fs + bit * (1 - 2 * (fs // bit % 2))}, device_id_type=MESH)
    for d in range(1, n_tp):
        pl.semaphore_signal(barrier, inc=1, device_id={"tp": lax.rem(tp + d, n_tp)}, device_id_type=MESH)
    pl.semaphore_wait(barrier, n_sp - 1 + len(bits) + n_tp - 1)


def gather_tokens(n_sp, n_tp, tokbuf, rows, tok_s, tok_r, halo_s, halo_r):
    sp, tp = lax.axis_index("sp"), lax.axis_index("tp")

    def tok_copy(d, owner):
        ref = tokbuf.at[pl.ds(pl.multiple_of(halo + owner * rows, 16), rows)]
        return pltpu.make_async_remote_copy(
            src_ref=ref, dst_ref=ref, send_sem=tok_s.at[d - 1], recv_sem=tok_r.at[d - 1],
            device_id={"tp": lax.rem(tp + d, n_tp)}, device_id_type=MESH)

    def halo_next():
        return pltpu.make_async_remote_copy(
            src_ref=tokbuf.at[pl.ds(n_tp * rows, halo)], dst_ref=tokbuf.at[pl.ds(0, halo)],
            send_sem=halo_s.at[0], recv_sem=halo_r.at[0],
            device_id={"sp": lax.rem(sp + 1, n_sp)}, device_id_type=MESH)

    def halo_side(d):
        ref = tokbuf.at[pl.ds(0, halo)]
        return pltpu.make_async_remote_copy(
            src_ref=ref, dst_ref=ref, send_sem=halo_s.at[d], recv_sem=halo_r.at[d],
            device_id={"tp": lax.rem(tp + d, n_tp)}, device_id_type=MESH)

    end = n_tp - 1

    def start():
        for d in range(1, n_tp):
            tok_copy(d, tp).start()

        @pl.when(jnp.logical_and(tp == end, sp < n_sp - 1))
        def _():
            halo_next().start()

        @pl.when(sp == 0)
        def _():
            tokbuf[0:halo, :] = jnp.zeros((halo, tokbuf.shape[1]), tokbuf.dtype)

    def finish():
        @pl.when(jnp.logical_and(tp == end, sp > 0))
        def _():
            halo_next().wait_recv()
            for d in range(1, n_tp):
                halo_side(d).start()
        for d in range(1, n_tp):
            tok_copy(d, lax.rem(tp - d + n_tp, n_tp)).wait_recv()

        @pl.when(jnp.logical_and(tp < end, sp > 0))
        def _():
            for d in range(1, n_tp):
                @pl.when(tp == d - 1)
                def _():
                    halo_side(d).wait_recv()

    def drain():
        for d in range(1, n_tp):
            tok_copy(d, tp).wait_send()

        @pl.when(jnp.logical_and(tp == end, sp < n_sp - 1))
        def _():
            halo_next().wait_send()

        @pl.when(jnp.logical_and(tp == end, sp > 0))
        def _():
            for d in range(1, n_tp):
                halo_side(d).wait_send()

    return start, finish, drain


def mixer_kernel(n_sp, n_fs, n_tp, *refs):
    tok_ref, gain_ref, wbd_ref, conv_ref, alog_ref, extra_ref, mix_ref, scale_ref, dgain_ref = refs[:9]
    w_refs = refs[9:16]
    out_ref = refs[16]
    (tokbuf, normbuf, wbuf, raw, pool_out, delta_out, pbuf, cbuf, s_in, s_out, part, rsbuf,
     loc, tok_s, tok_r, halo_s, halo_r, z_s, z_r, f_s, f_r, st_s, st_r, rs_s, rs_r) = refs[17:]
    rows, width = tok_ref.shape
    length = n_tp * rows
    heads, head_dim = cbuf.shape[0], cbuf.shape[1]
    groups, group_dim = mix_ref.shape[0], mix_ref.shape[1]
    sp, tp = lax.axis_index("sp"), lax.axis_index("tp")
    count = len(w_refs)
    local = [pltpu.make_async_copy(w_refs[i], wbuf.at[i, sp], loc.at[i]) for i in range(count)]
    here = pltpu.make_async_copy(
        tok_ref, tokbuf.at[pl.ds(pl.multiple_of(halo + tp * rows, 16), rows)], loc.at[count])
    here.start()
    for copy in local:
        copy.start()
    enter(n_sp, n_fs, n_tp)
    start, finish, drain = gather_tokens(n_sp, n_tp, tokbuf, rows, tok_s, tok_r, halo_s, halo_r)
    gather = Gather(n_sp, n_fs, wbuf, z_s, z_r, f_s, f_r)
    here.wait()
    start()
    for w in range(count):
        local[w].wait()
        if w < AHEAD:
            gather.send(w)
    depth = wbuf.shape[2]

    def norm(i, c):
        at = pl.ds(pl.multiple_of(i * 16, 16), 16)
        normbuf[at, :] = rms_rows(tokbuf[at, :], gain_ref[...])
        return c

    def project(w):
        total = None
        for s in range(n_sp):
            term = jnp.dot(normbuf[:, s * depth:(s + 1) * depth], wbuf[w, s], preferred_element_type=f32)
            total = term if total is None else total + term
        raw[w] = total.astype(bf16).astype(f32)

    gather.forward(0)
    gather.forward(1)
    finish()
    lax.fori_loop(0, tokbuf.shape[0] // 16, norm, 0)
    pre = jnp.dot(normbuf[...], wbd_ref[...], preferred_element_type=f32)[halo:]
    softplus = jnp.maximum(pre, 0.0) + jnp.log1p(jnp.exp(-jnp.abs(pre)))
    log_gate = -jnp.exp(alog_ref[...]) * softplus + extra_ref[...]
    strength = jax.nn.sigmoid(pre)
    row = lax.broadcasted_iota(jnp.int32, (length, length), 0)
    col = lax.broadcasted_iota(jnp.int32, (length, length), 1)
    tri = jnp.where((row // BLOCK == col // BLOCK) & (row >= col), 1.0, 0.0)
    cum = mm(tri, log_gate)
    cum_t = cum.T

    gather.finish(0)
    project(0)
    gather.forward(2)
    gather.finish(1)
    project(1)
    gather.forward(3)
    gather.finish(2)
    project(2)

    def active(role, w, h):
        at = slice(h * head_dim, (h + 1) * head_dim)
        taps = conv_ref.shape[1]
        total = None
        for j in range(taps):
            term = raw[w, pl.ds(halo - (taps - 1) + j, length), at] * conv_ref[role, j:j + 1, at]
            total = term if total is None else total + term
        return silu(total)

    unit = min(PAIR, length)
    i2 = lax.broadcasted_iota(jnp.int32, (unit, unit), 0)
    j2 = lax.broadcasted_iota(jnp.int32, (unit, unit), 1)
    lower = (i2 // BLOCK == j2 // BLOCK) & (i2 >= j2)
    strict = lower & (i2 > j2)
    eye = jnp.where(i2 == j2, 1.0, 0.0)

    def delta(some):
        units = []
        for h in some:
            q = unit_rows(active(0, QUERY, h)) * head_dim ** (-0.5)
            k = unit_rows(active(1, KEY, h))
            v = active(2, VALUE, h)
            beta = strength[:, heads + h:heads + h + 1]
            g = cum[:, h:h + 1]
            grow = jnp.exp(g)
            kb = k * beta
            right = jnp.concatenate([v * beta, kb * grow], axis=1)
            qg = q * grow
            for p in range(length // unit):
                at = slice(p * unit, (p + 1) * unit)
                gaps = g[at] - cum_t[h:h + 1, at]
                decay = jnp.where(lower, jnp.exp(jnp.where(lower, gaps, 0.0)), 0.0)
                both = mm(jnp.concatenate([kb[at], q[at]], axis=0), k[at], ((1,), (1,)))
                corr = jnp.where(strict, both[:unit] * decay, 0.0)
                scores = both[unit:] * decay
                units.append([h, p, corr, scores, right[at], qg[at], k[at], g[at]])
        done = [eye - jnp.where((i2 // 2 == j2 // 2), u[2], 0.0) for u in units]
        size = 2
        while size < BLOCK:
            pair = (i2 // (2 * size) == j2 // (2 * size)) & (i2 // size != j2 // size)
            half = [mm(jnp.where(pair, u[2], 0.0), x) for u, x in zip(units, done)]
            done = [x - mm(x, y) for x, y in zip(done, half)]
            size *= 2
        solved = [mm(x, u[4]) for u, x in zip(units, done)]
        carry = {h: jnp.concatenate([jnp.where(
            lax.broadcasted_iota(jnp.int32, (head_dim, head_dim), 0)
            == lax.broadcasted_iota(jnp.int32, (head_dim, head_dim), 1), 1.0, 0.0),
            jnp.zeros((head_dim, head_dim), f32)], axis=1) for h in some}
        per = length // unit
        for p in range(per):
            for b in range(unit // BLOCK):
                at = slice(b * BLOCK, (b + 1) * BLOCK)
                for n, h in enumerate(some):
                    _, _, _, scores, _, qg, k, g = units[n * per + p]
                    fixed = solved[n * per + p][at, :head_dim]
                    kw = solved[n * per + p][at, head_dim:]
                    last = g[(b + 1) * BLOCK - 1:(b + 1) * BLOCK]
                    fall = k[at] * jnp.exp(last - g[at])
                    c = carry[h]
                    two = mm(jnp.concatenate([kw, qg[at]], axis=0), c, precision=None)
                    fresh = jnp.concatenate([jnp.zeros_like(fixed), fixed], axis=1) - two[:BLOCK]
                    pbuf[h, p * unit + b * BLOCK:p * unit + (b + 1) * BLOCK, :] = (
                        two[BLOCK:] + mm(scores[at, at], fresh, precision=None))
                    carry[h] = jnp.exp(last) * c + mm(fall, fresh, ((0,), (0,)), None)
        for h in some:
            cbuf[h] = carry[h]

    def pool():
        at_row = lax.broadcasted_iota(jnp.int32, (length, group_dim), 0) + sp * length
        for i in range(groups):
            at = slice(i * group_dim, (i + 1) * group_dim)
            x = raw[POOL, :, at]
            span = 2 * jnp.left_shift(1, lax.rem(tp * groups + i, 4))
            total = x
            window = jnp.zeros_like(x)
            for w in (2, 4, 8, 16):
                total = total + pltpu.roll(total, w // 2, 0)
                window = window + jnp.where(span == w, total, 0.0)
            tally = jnp.minimum(at_row + 1, span).astype(f32)
            pooled = (window[halo:] / tally - x[halo:]).astype(bf16)
            mixed = jnp.dot(pooled, mix_ref[i], preferred_element_type=f32)
            pool_out[:, at] = (mixed * scale_ref[:, at]).astype(bf16)

    cut = (heads + 1) // 2
    delta(range(cut))
    gather.forward(4)
    gather.finish(3)
    project(3)
    if cut < heads:
        delta(range(cut, heads))
    gather.forward(5)
    gather.finish(4)
    project(4)

    def state_copy(h):
        return pltpu.make_async_remote_copy(
            src_ref=s_out.at[h], dst_ref=s_in.at[h], send_sem=st_s.at[h], recv_sem=st_r.at[h],
            device_id={"sp": lax.rem(sp + 1, n_sp)}, device_id_type=MESH)

    @pl.when(sp == 0)
    def _():
        s_in[...] = jnp.zeros_like(s_in)

    gather.forward(6)
    gather.finish(5)
    pool()
    for h in range(heads):
        @pl.when(sp > 0)
        def _():
            state_copy(h).wait_recv()
        s_out[h] = (mm(cbuf[h, :, :head_dim], s_in[h].astype(f32), precision=None) + cbuf[h, :, head_dim:]).astype(bf16)

        @pl.when(sp < n_sp - 1)
        def _():
            state_copy(h).start()
    gather.flush(6)
    for h in range(heads):
        at = slice(h * head_dim, (h + 1) * head_dim)
        attended = mm(pbuf[h, :, :head_dim], s_in[h].astype(f32), precision=None) + pbuf[h, :, head_dim:]
        scale = lax.rsqrt(jnp.mean(attended * attended, axis=-1, keepdims=True) + eps)
        delta_out[:, at] = (attended * scale * dgain_ref[...] * silu(raw[GATE, halo:, at])).astype(bf16)
    gather.finish(6)

    def rs_copy(s, d, owner, dest):
        return pltpu.make_async_remote_copy(
            src_ref=part.at[s, pl.ds(pl.multiple_of(dest * rows, 16), rows)], dst_ref=rsbuf.at[s, owner],
            send_sem=rs_s.at[s, d - 1], recv_sem=rs_r.at[s, d - 1],
            device_id={"tp": lax.rem(tp + d, n_tp)}, device_id_type=MESH)

    for s in range(n_sp):
        part[s] = (jnp.dot(pool_out[...], wbuf[OUT_POOL, s], preferred_element_type=f32)
                   + jnp.dot(delta_out[...], wbuf[OUT_DELTA, s], preferred_element_type=f32)).astype(bf16)
        for d in range(1, n_tp):
            rs_copy(s, d, tp, lax.rem(tp + d, n_tp)).start()
    cols = wbuf.shape[3]
    for s in range(n_sp):
        total = part[s, pl.ds(pl.multiple_of(tp * rows, 16), rows)].astype(f32)
        for d in range(1, n_tp):
            owner = lax.rem(tp - d + n_tp, n_tp)
            rs_copy(s, d, owner, tp).wait_recv()
            total = total + rsbuf[s, owner].astype(f32)
        out_ref[:, s * cols:(s + 1) * cols] = total.astype(bf16)
    drain()
    for w in range(count):
        gather.drain(w)

    @pl.when(sp < n_sp - 1)
    def _():
        for h in range(heads):
            state_copy(h).wait_send()
    for s in range(n_sp):
        for d in range(1, n_tp):
            rs_copy(s, d, tp, lax.rem(tp + d, n_tp)).wait_send()


def per_device(
    tokens,
    norm_gain,
    w_pool_in,
    w_query,
    w_key,
    w_value,
    w_gate,
    w_beta,
    w_decay,
    conv_weight,
    a_log,
    decay_extra,
    w_mix,
    pool_scale,
    delta_gain,
    w_out_pool,
    w_out_delta,
):
    n_sp, n_fs, n_tp = (lax.axis_size(a) for a in ("sp", "fs", "tp"))
    weights = (w_key, w_query, w_value, w_pool_in, w_gate, w_out_pool, w_out_delta)
    rows, width = tokens.shape
    depth, cols = w_key.shape
    heads = a_log.shape[0]
    head_dim = cols // heads
    length = n_tp * rows
    count = len(weights)
    lanes = 128
    lane = lax.axis_index("tp")

    def own(w):
        return lax.dynamic_slice_in_dim(w, lane * heads, heads, 1)

    def wide(x):
        return jnp.pad(x, ((0, 0), (0, lanes - x.shape[1])))

    w_bd = wide(jnp.concatenate([own(w_decay), own(w_beta)], axis=1))
    slots = max(1, 2 ** len(share_bits(n_fs)) - 1)
    side = max(1, n_tp - 1)
    dma = pltpu.SemaphoreType.DMA
    vmem, anywhere = pl.BlockSpec(memory_space=pltpu.VMEM), pl.BlockSpec(memory_space=pl.ANY)
    return pl.pallas_call(
        functools.partial(mixer_kernel, n_sp, n_fs, n_tp),
        out_shape=jax.ShapeDtypeStruct((rows, width), bf16),
        in_specs=[anywhere] + [vmem] * 8 + [anywhere] * count,
        out_specs=vmem,
        scratch_shapes=[
            pltpu.VMEM((halo + length, width), bf16),
            pltpu.VMEM((halo + length, width), bf16),
            pltpu.VMEM((count, n_sp, depth, cols), bf16),
            pltpu.VMEM((5, halo + length, cols), f32),
            pltpu.VMEM((length, cols), bf16),
            pltpu.VMEM((length, cols), bf16),
            pltpu.VMEM((heads, length, 2 * head_dim), f32),
            pltpu.VMEM((heads, head_dim, 2 * head_dim), f32),
            pltpu.VMEM((heads, head_dim, head_dim), bf16),
            pltpu.VMEM((heads, head_dim, head_dim), bf16),
            pltpu.VMEM((n_sp, length, cols), bf16),
            pltpu.VMEM((n_sp, n_tp, rows, cols), bf16),
            dma((count + 1,)), dma((side,)), dma((side,)), dma((n_tp,)), dma((n_tp,)),
            dma((count, n_sp, 2)), dma((count, n_sp)), dma((count, n_sp, slots)), dma((count, n_sp, slots)),
            dma((heads,)), dma((heads,)), dma((n_sp, side)), dma((n_sp, side)),
        ],
        compiler_params=pltpu.CompilerParams(collective_id=0, has_side_effects=True, vmem_limit_bytes=56 << 20),
    )(tokens, norm_gain.reshape(1, -1), w_bd, conv_weight, wide(a_log.reshape(1, -1)), wide(decay_extra), w_mix,
      pool_scale.reshape(1, -1), delta_gain.reshape(1, -1), *weights)


def solution(mesh):
    placed = (
        P(("fs", "sp", "tp"), None),
        P(),
        P("sp", "tp"),
        P("sp", "tp"),
        P("sp", "tp"),
        P("sp", "tp"),
        P("sp", "tp"),
        P(),
        P(),
        P(None, None, "tp"),
        P("tp"),
        P(("fs", "sp"), "tp"),
        P("tp", None, None),
        P("tp"),
        P(),
        P("tp", "sp"),
        P("tp", "sp"),
    )
    return jax.shard_map(
        per_device,
        mesh=mesh,
        in_specs=placed,
        out_specs=P(("fs", "sp", "tp"), None),
        check_vma=False,
    )
```

profile of v0, /device:TPU:31, one launch (start us, length us, event | category | flops | bytes accessed | tf_op | source)
XLA Modules:
  0.0 135.7 jit_solution(8396402994204324408)
XLA Ops:
  0.0 0.0 copy-start
  0.0 1.2 pad.13.refs_4_
  1.2 1.3 reshape.12.refs_1_
  2.5 0.0 copy-done
  2.5 0.8 constant_dynamic-slice_fusion
  3.3 0.0 copy-start.1
  3.3 0.6 copy-done.1
  4.0 0.1 copy.22
  4.1 0.7 pad.14.refs_5_
  4.8 0.3 copy.21
  5.1 0.9 pad.12.refs_2_
  6.0 127.9 %shard_map.163 = bf16[128,2048]{1,0:T(8,128)(2,1)} custom-call(bf16[128,2048]{1,0:T(8,128)(2,1)} %refs_0_.1, bf16[1,2048]{1,0:T(2,128)(2,1)} %reshape.12.refs_1_, bf16[2048,128]{1,0:T(8,128)(2,1)} %pad.12.refs_2_, f32[3,4,512]{2,1,0:T(4,128)} %refs_3_.1, f32[1,128]{1,0:T(1,128)} %pad.13.refs_4_, f32[256,128]{1,0:T(8,128)} %pad.14.refs_5_, ...), custom_call_target="tpu_custom_call" | custom-call | tf_op jit(solution)/shard_map/pallas_call | solution.py:505
  133.8 1.9 %copy.24 = bf16[128,2048]{1,0:T(8,128)(2,1)} copy(bf16[128,2048]{1,0:T(8,128)(2,1)} %shard_map.163) | data formatting | bytes 1048576
  (1 shorter events, 0.0 us)
Async XLA Ops:
  0.0 2.5 %copy-start = (bf16[2048,8]{0,1:T(8,128)(2,1)S(1)}, bf16[2048,8]{0,1:T(8,128)(2,1)}, u32[]{:S(2)}) copy-start(bf16[2048,8]{0,1:T(8,128)(2,1)} %param.24) | copy-start | bytes 98308
  3.3 0.7 copy-start.1
where the time goes:
time: 136 us
  Pallas kernels  128 us (94%)
  local copies, waits for them, and re-layouts  7.79 us (6%)
    pallas_call x1, Pallas kernels, per_device(): pl.pallas_call(functools.partial(mixer_kernel, n_sp, n_fs, n_tp), out_sha...  128 us
    pad x3, local copies, waits for them, and re-layouts, wide(): return jnp.pad(x, ((0, 0), (0, lanes - x.shape[1])))  2.78 us

commit v1 on v0

v1 whole, which is shorter than its diff:
```python
import functools

import jax
import jax.numpy as jnp
from jax import lax
from jax.experimental import pallas as pl
from jax.experimental.pallas import tpu as pltpu
from jax.sharding import PartitionSpec as P

BLOCK = 64
PAIR = 2 * BLOCK

eps = 1e-06
halo = 16
MESH = pl.DeviceIdType.MESH
highest = lax.Precision.HIGHEST
f32 = jnp.float32
bf16 = jnp.bfloat16
KEY, QUERY, VALUE, POOL, GATE, OUT_POOL, OUT_DELTA = range(7)
AHEAD = 2
LAG = 2
UNROLL = 32


def mm(a, b, dims=((1,), (0,)), precision=highest):
    return lax.dot_general(a, b, (dims, ((), ())), precision=precision, preferred_element_type=f32)


def rms_rows(values, gain):
    floats = values.astype(f32)
    scale = lax.rsqrt(jnp.mean(floats * floats, axis=-1, keepdims=True) + eps)
    return (floats * scale * gain.astype(f32)).astype(bf16)


def unit_rows(values):
    return values * lax.rsqrt(jnp.sum(values * values, axis=-1, keepdims=True) + eps)


def silu(x):
    return x * jax.nn.sigmoid(x)


def share_bits(n_fs):
    if n_fs & (n_fs - 1):
        return []
    return [n_fs >> (k + 1) for k in range(n_fs.bit_length() - 1)]


def both(a, b):
    if isinstance(a, bool):
        return b if a else False
    if isinstance(b, bool):
        return a if b else False
    return jnp.logical_and(a, b)


def when(cond, act):
    if isinstance(cond, bool):
        if cond:
            act()
    else:
        pl.when(cond)(act)


class Gather:
    def __init__(self, n_sp, n_fs, wbuf, z_s, z_f, z_r, f_s, f_r, last_r):
        self.n_sp, self.bits = n_sp, share_bits(n_fs)
        self.wbuf, self.z_s, self.z_f, self.z_r, self.f_s, self.f_r, self.last_r = wbuf, z_s, z_f, z_r, f_s, f_r, last_r
        self.sp, self.fs = lax.axis_index("sp"), lax.axis_index("fs")
        self.count = wbuf.shape[0]
        self.span = n_sp - 1
        self.pieces = 2 ** len(self.bits)
        self.mine = self.fs if self.bits else 0 * self.fs
        self.depth = wbuf.shape[2] // self.pieces

    def partner(self, bit):
        return self.fs + bit * (1 - 2 * (self.fs // bit % 2))

    def mask_of(self, m, index):
        for i, bit in enumerate(self.bits):
            if m >> i & 1:
                index = index + bit * (1 - 2 * (index // bit % 2))
        return index

    def piece(self, w, src, index):
        return self.wbuf.at[w, src, pl.ds(pl.multiple_of(index * self.depth, self.depth), self.depth)]

    def z_copy(self, w, src, way, own):
        ref = self.piece(w, src, self.mine)
        to = lax.rem(self.sp + way + self.n_sp, self.n_sp)
        sent = self.z_s.at[w, (way + 1) // 2] if own else self.z_f.at[w]
        return pltpu.make_async_remote_copy(
            src_ref=ref, dst_ref=ref, send_sem=sent, recv_sem=self.z_r.at[w, src],
            device_id={"sp": to}, device_id_type=MESH)

    def f_copy(self, w, src, k, m):
        ref = self.piece(w, src, self.mask_of(m, self.mine))
        inner = k < len(self.bits) - 1
        return pltpu.make_async_remote_copy(
            src_ref=ref, dst_ref=ref, send_sem=self.f_s.at[w],
            recv_sem=self.f_r.at[w, src, 2 ** k - 1 + m] if inner else self.last_r.at[w, src],
            device_id={"fs": self.partner(self.bits[k])}, device_id_type=MESH)

    def can_send(self, way):
        return self.sp < self.n_sp - 1 if way == 1 else self.sp > 0

    def send(self, w):
        for way in (1, -1):
            @pl.when(self.can_send(way))
            def _():
                self.z_copy(w, self.sp, way, True).start()

    def each(self, t, act):
        for way in (1, -1):
            src = self.sp - way * t
            @pl.when(src >= 0 if way == 1 else src < self.n_sp)
            def _():
                act(src, way)

    def arrive_z(self, w, src, way):
        self.z_copy(w, src, way, False).wait_recv()

        @pl.when(self.can_send(way))
        def _():
            self.z_copy(w, src, way, False).start()
        for k in range(len(self.bits)):
            self.f_copy(w, src, k, 0).start()

    def arrive_f(self, w, t, k):
        def act(src, way):
            for m in range(2 ** k):
                self.f_copy(w, src, k, m).wait_recv()
                for later in range(k + 1, len(self.bits)):
                    self.f_copy(w, src, later, m | 1 << k).start()
        self.each(t, act)

    def steps(self):
        return self.count * self.span

    def step(self, i):
        w, t = i // self.span, i % self.span + 1
        when(i < self.steps(), lambda: self.each(t, lambda src, way: self.arrive_z(w, src, way)))
        when(both(t == 1, w + AHEAD < self.count), lambda: self.send(w + AHEAD))
        for k in range(len(self.bits) - 1):
            j = i - LAG * (k + 1)
            when(both(j >= 0, j < self.steps()), lambda: self.arrive_f(j // self.span, j % self.span + 1, k))

    def end(self):
        return self.steps() + LAG * max(0, len(self.bits) - 1)

    def ready(self, w, t):
        if self.bits:
            def act(src, way):
                ref = self.wbuf.at[w, src, pl.ds(0, self.wbuf.shape[2] // 2)]
                pltpu.make_async_copy(ref, ref, self.last_r.at[w, src]).wait()
            self.each(t, act)

    def finish(self, w):
        self.loop(1, self.n_sp, lambda t: self.ready(w, t))

    def drain(self, w):
        for way in (1, -1):
            @pl.when(self.can_send(way))
            def _():
                self.z_copy(w, self.sp, way, True).wait_send()
        if self.n_sp > 2:
            @pl.when(jnp.logical_and(self.can_send(1), self.can_send(-1)))
            def _():
                ref = self.wbuf.at[w, pl.ds(0, self.span), pl.ds(0, self.depth)]
                pltpu.make_async_copy(ref, ref, self.z_f.at[w]).wait()
        if self.bits:
            ref = self.wbuf.at[w, pl.ds(0, self.span), pl.ds(0, (self.pieces - 1) * self.depth)]
            pltpu.make_async_copy(ref, ref, self.f_s.at[w]).wait()

    def loop(self, a, b, act):
        if self.steps() <= UNROLL:
            for i in range(a, b):
                act(i)
        else:
            def body(i, c):
                act(i)
                return c
            lax.fori_loop(a, b, body, 0)


def enter(n_sp, n_fs, n_tp):
    sp, fs, tp = (lax.axis_index(a) for a in ("sp", "fs", "tp"))
    barrier = pltpu.get_barrier_semaphore()
    bits = share_bits(n_fs)

    def greet(where):
        pl.semaphore_signal(barrier, inc=1, device_id=where, device_id_type=MESH)
    right, left = sp < n_sp - 1, sp > 0
    pl.when(right)(lambda: greet({"sp": lax.rem(sp + 1, n_sp)}))
    pl.when(left)(lambda: greet({"sp": lax.rem(sp + n_sp - 1, n_sp)}))
    for bit in bits:
        greet({"fs": fs + bit * (1 - 2 * (fs // bit % 2))})
    for d in range(1, n_tp):
        greet({"tp": lax.rem(tp + d, n_tp)})
    heard = len(bits) + n_tp - 1
    pl.semaphore_wait(barrier, heard + right.astype(jnp.int32) + left.astype(jnp.int32))


class Tokens:
    def __init__(self, n_sp, n_tp, tokbuf, rows, tok_s, tok_r, halo_s, halo_r):
        self.n_sp, self.n_tp, self.tokbuf, self.rows = n_sp, n_tp, tokbuf, rows
        self.tok_s, self.tok_r, self.halo_s, self.halo_r = tok_s, tok_r, halo_s, halo_r
        self.sp, self.tp = lax.axis_index("sp"), lax.axis_index("tp")
        self.end = n_tp - 1

    def tok_copy(self, d, owner):
        ref = self.tokbuf.at[pl.ds(pl.multiple_of(halo + owner * self.rows, 16), self.rows)]
        return pltpu.make_async_remote_copy(
            src_ref=ref, dst_ref=ref, send_sem=self.tok_s.at[d - 1], recv_sem=self.tok_r.at[d - 1],
            device_id={"tp": lax.rem(self.tp + d, self.n_tp)}, device_id_type=MESH)

    def halo_next(self):
        return pltpu.make_async_remote_copy(
            src_ref=self.tokbuf.at[pl.ds(self.n_tp * self.rows, halo)], dst_ref=self.tokbuf.at[pl.ds(0, halo)],
            send_sem=self.halo_s.at[0], recv_sem=self.halo_r.at[0],
            device_id={"sp": lax.rem(self.sp + 1, self.n_sp)}, device_id_type=MESH)

    def halo_side(self, d):
        ref = self.tokbuf.at[pl.ds(0, halo)]
        return pltpu.make_async_remote_copy(
            src_ref=ref, dst_ref=ref, send_sem=self.halo_s.at[d], recv_sem=self.halo_r.at[d],
            device_id={"tp": lax.rem(self.tp + d, self.n_tp)}, device_id_type=MESH)

    def start(self):
        for d in range(1, self.n_tp):
            self.tok_copy(d, self.tp).start()

    def start_halo(self):
        @pl.when(jnp.logical_and(self.tp == self.end, self.sp < self.n_sp - 1))
        def _():
            self.halo_next().start()

        @pl.when(self.sp == 0)
        def _():
            self.tokbuf[0:halo, :] = jnp.zeros((halo, self.tokbuf.shape[1]), self.tokbuf.dtype)

    def relay(self):
        @pl.when(jnp.logical_and(self.tp == self.end, self.sp > 0))
        def _():
            self.halo_next().wait_recv()
            for d in range(1, self.n_tp):
                self.halo_side(d).start()

    def finish(self):
        for d in range(1, self.n_tp):
            self.tok_copy(d, lax.rem(self.tp - d + self.n_tp, self.n_tp)).wait_recv()

        @pl.when(jnp.logical_and(self.tp < self.end, self.sp > 0))
        def _():
            for d in range(1, self.n_tp):
                @pl.when(self.tp == d - 1)
                def _():
                    self.halo_side(d).wait_recv()

    def drain(self):
        for d in range(1, self.n_tp):
            self.tok_copy(d, self.tp).wait_send()

        @pl.when(jnp.logical_and(self.tp == self.end, self.sp < self.n_sp - 1))
        def _():
            self.halo_next().wait_send()

        @pl.when(jnp.logical_and(self.tp == self.end, self.sp > 0))
        def _():
            for d in range(1, self.n_tp):
                self.halo_side(d).wait_send()


def mixer_kernel(n_sp, n_fs, n_tp, *refs):
    tok_ref, gain_ref, wbd_ref, conv_ref, alog_ref, extra_ref, mix_ref, scale_ref, dgain_ref = refs[:9]
    w_refs = refs[9:16]
    out_ref = refs[16]
    (tokbuf, normbuf, wbuf, raw, pool_out, delta_out, pbuf, cbuf, s_in, s_out, part, rsbuf,
     kbuf, xbuf, kwbuf, fbuf, qbuf, sbuf, gbuf, acc,
     loc, tok_s, tok_r, halo_s, halo_r, z_s, z_f, z_r, f_s, f_r, last_r, st_s, st_r, rs_s, rs_r) = refs[17:]
    rows, width = tok_ref.shape
    length = n_tp * rows
    heads, head_dim = cbuf.shape[0], cbuf.shape[1]
    groups, group_dim = mix_ref.shape[0], mix_ref.shape[1]
    sp, tp = lax.axis_index("sp"), lax.axis_index("tp")
    count = len(w_refs)
    cols = wbuf.shape[3]
    depth = wbuf.shape[2]
    local = [pltpu.make_async_copy(w_refs[i], wbuf.at[i, sp], loc.at[i]) for i in range(count)]
    here = pltpu.make_async_copy(
        tok_ref, tokbuf.at[pl.ds(pl.multiple_of(halo + tp * rows, 16), rows)], loc.at[count])
    local[0].start()
    here.start()
    for copy in local[1:]:
        copy.start()
    enter(n_sp, n_fs, n_tp)
    tokens = Tokens(n_sp, n_tp, tokbuf, rows, tok_s, tok_r, halo_s, halo_r)
    gather = Gather(n_sp, n_fs, wbuf, z_s, z_f, z_r, f_s, f_r, last_r)
    span = gather.span
    local[0].wait()
    gather.send(0)
    here.wait()
    tokens.start()
    for w in range(1, count):
        local[w].wait()
        if w < AHEAD:
            gather.send(w)
    tokens.start_halo()

    def norm(a, b):
        def body(i, c):
            at = pl.ds(pl.multiple_of(i * 16, 16), 16)
            normbuf[at, :] = rms_rows(tokbuf[at, :], gain_ref[...])
            return c
        lax.fori_loop(a, b, body, 0)

    def project(w):
        total = None
        for s in range(n_sp):
            term = jnp.dot(normbuf[:, s * depth:(s + 1) * depth], wbuf[w, s], preferred_element_type=f32)
            total = term if total is None else total + term
        raw[w] = total.astype(bf16).astype(f32)

    def active(role, w, h):
        at = slice(h * head_dim, (h + 1) * head_dim)
        taps = conv_ref.shape[1]
        total = None
        for j in range(taps):
            term = raw[w, pl.ds(halo - (taps - 1) + j, length), at] * conv_ref[role, j:j + 1, at]
            total = term if total is None else total + term
        return silu(total)

    unit = min(PAIR, length)
    per = length // unit
    i2 = lax.broadcasted_iota(jnp.int32, (unit, unit), 0)
    j2 = lax.broadcasted_iota(jnp.int32, (unit, unit), 1)
    lower = (i2 // BLOCK == j2 // BLOCK) & (i2 >= j2)
    strict = lower & (i2 > j2)

    def gates():
        pre = jnp.dot(normbuf[...], wbd_ref[...], preferred_element_type=f32)[halo:]
        softplus = jnp.maximum(pre, 0.0) + jnp.log1p(jnp.exp(-jnp.abs(pre)))
        log_gate = -jnp.exp(alog_ref[...]) * softplus + extra_ref[...]
        row = lax.broadcasted_iota(jnp.int32, (length, length), 0)
        col = lax.broadcasted_iota(jnp.int32, (length, length), 1)
        tri = jnp.where((row // BLOCK == col // BLOCK) & (row >= col), 1.0, 0.0)
        cum = mm(tri, log_gate)
        gbuf[0] = jax.nn.sigmoid(pre)
        gbuf[1] = cum
        cum_t = cum.T
        for p in range(per):
            for h in range(heads):
                at = slice(p * unit, (p + 1) * unit)
                gaps = cum[at, h:h + 1] - cum_t[h:h + 1, at]
                sbuf[h, p] = jnp.where(lower, jnp.exp(jnp.where(lower, gaps, 0.0)), 0.0)

    def keys(some):
        eye = jnp.where(i2 == j2, 1.0, 0.0)
        units = []
        for h in some:
            k = unit_rows(active(1, KEY, h))
            kb = k * gbuf[0, :, heads + h:heads + h + 1]
            kbuf[h] = k
            for p in range(per):
                at = slice(p * unit, (p + 1) * unit)
                corr = jnp.where(strict, mm(kb[at], k[at], ((1,), (1,))) * sbuf[h, p], 0.0)
                units.append((h, p, corr))
            kwbuf[h] = kb * jnp.exp(gbuf[1, :, h:h + 1])
        done = [eye - jnp.where(i2 // 2 == j2 // 2, u[2], 0.0) for u in units]
        size = 2
        while size < BLOCK:
            pair = (i2 // (2 * size) == j2 // (2 * size)) & (i2 // size != j2 // size)
            half = [mm(jnp.where(pair, u[2], 0.0), x) for u, x in zip(units, done)]
            done = [x - mm(x, y) for x, y in zip(done, half)]
            size *= 2
        for (h, p, _), x in zip(units, done):
            at = slice(p * unit, (p + 1) * unit)
            xbuf[h, p] = x
            kwbuf[h, at] = mm(x, kwbuf[h, at])

    def queries(some):
        for h in some:
            q = unit_rows(active(0, QUERY, h)) * head_dim ** (-0.5)
            qbuf[h] = q * jnp.exp(gbuf[1, :, h:h + 1])
            for p in range(per):
                at = slice(p * unit, (p + 1) * unit)
                sbuf[h, p] = mm(q[at], kbuf[h, at], ((1,), (1,))) * sbuf[h, p]

    def values(some):
        for h in some:
            vb = active(2, VALUE, h) * gbuf[0, :, heads + h:heads + h + 1]
            for p in range(per):
                at = slice(p * unit, (p + 1) * unit)
                fbuf[h, at] = mm(xbuf[h, p], vb[at])

    def scan():
        blank = jnp.concatenate([jnp.where(
            lax.broadcasted_iota(jnp.int32, (head_dim, head_dim), 0)
            == lax.broadcasted_iota(jnp.int32, (head_dim, head_dim), 1), 1.0, 0.0),
            jnp.zeros((head_dim, head_dim), f32)], axis=1)
        for p in range(per):
            for b in range(unit // BLOCK):
                at = slice(p * unit + b * BLOCK, p * unit + (b + 1) * BLOCK)
                sub = slice(b * BLOCK, (b + 1) * BLOCK)
                for h in range(heads):
                    fixed = fbuf[h, at]
                    g = gbuf[1, at, h:h + 1]
                    last = g[BLOCK - 1:BLOCK]
                    fall = kbuf[h, at] * jnp.exp(last - g)
                    c = blank if p + b == 0 else cbuf[h]
                    two = mm(jnp.concatenate([kwbuf[h, at], qbuf[h, at]], axis=0), c, precision=None)
                    fresh = jnp.concatenate([jnp.zeros_like(fixed), fixed], axis=1) - two[:BLOCK]
                    pbuf[h, at, :] = two[BLOCK:] + mm(sbuf[h, p, sub, sub], fresh, precision=None)
                    cbuf[h] = jnp.exp(last) * c + mm(fall, fresh, ((0,), (0,)), None)

    def pool():
        at_row = lax.broadcasted_iota(jnp.int32, (length, group_dim), 0) + sp * length
        for i in range(groups):
            at = slice(i * group_dim, (i + 1) * group_dim)
            x = raw[POOL, :, at]
            span_of = 2 * jnp.left_shift(1, lax.rem(tp * groups + i, 4))
            total = x
            window = jnp.zeros_like(x)
            for w in (2, 4, 8, 16):
                total = total + pltpu.roll(total, w // 2, 0)
                window = window + jnp.where(span_of == w, total, 0.0)
            tally = jnp.minimum(at_row + 1, span_of).astype(f32)
            pooled = (window[halo:] / tally - x[halo:]).astype(bf16)
            mixed = jnp.dot(pooled, mix_ref[i], preferred_element_type=f32)
            pool_out[:, at] = (mixed * scale_ref[:, at]).astype(bf16)

    def state_copy(h):
        return pltpu.make_async_remote_copy(
            src_ref=s_out.at[h], dst_ref=s_in.at[h], send_sem=st_s.at[h], recv_sem=st_r.at[h],
            device_id={"sp": lax.rem(sp + 1, n_sp)}, device_id_type=MESH)

    def relay():
        for h in range(heads):
            @pl.when(sp > 0)
            def _():
                state_copy(h).wait_recv()

            @pl.when(sp < n_sp - 1)
            def _():
                s_out[h] = (mm(cbuf[h, :, :head_dim], s_in[h].astype(f32), precision=None)
                            + cbuf[h, :, head_dim:]).astype(bf16)
                state_copy(h).start()

    def attend():
        for h in range(heads):
            at = slice(h * head_dim, (h + 1) * head_dim)
            attended = mm(pbuf[h, :, :head_dim], s_in[h].astype(f32), precision=None) + pbuf[h, :, head_dim:]
            scale = lax.rsqrt(jnp.mean(attended * attended, axis=-1, keepdims=True) + eps)
            delta_out[:, at] = (attended * scale * dgain_ref[...] * silu(raw[GATE, halo:, at])).astype(bf16)

    first = 4 * span

    def turn(r):
        return first + 7 * r // 3

    def plain(i):
        gather.step(i)

    def relaying(i):
        gather.step(i)
        if isinstance(i, int):
            for r in range(n_sp):
                if turn(r) == i:
                    pl.when(sp == r)(relay)
        else:
            pl.when(i == turn(sp))(relay)

    def advance(a, b):
        gather.loop(a, b, plain)

    half = (heads + 1) // 2
    low = halo // 16 + tp * (rows // 16)
    high = low + rows // 16
    first_part, second_part = range(half), range(half, heads)

    @pl.when(sp == 0)
    def _():
        s_in[...] = jnp.zeros_like(s_in)
    advance(0, 1)
    norm(low, high)
    advance(1, span)
    tokens.relay()
    advance(span, span + 1)
    tokens.finish()
    norm(0, low)
    norm(high, tokbuf.shape[0] // 16)
    gates()
    at = span + LAG
    advance(span + 1, at)
    gather.finish(KEY)
    project(KEY)
    keys(first_part)
    advance(at, at + 1)
    keys(second_part)
    advance(at + 1, 2 * span + LAG)
    gather.finish(QUERY)
    project(QUERY)
    queries(range(heads))
    gather.drain(KEY)
    advance(2 * span + LAG, 3 * span + LAG)
    gather.finish(VALUE)
    project(VALUE)
    values(range(heads))
    gather.drain(QUERY)
    scan()
    gather.loop(3 * span + LAG, 4 * span + LAG, relaying)
    gather.finish(POOL)
    project(POOL)
    pool()
    gather.drain(VALUE)
    gather.loop(4 * span + LAG, 5 * span + LAG, relaying)
    gather.finish(GATE)
    project(GATE)
    gather.drain(POOL)
    tokens.drain()
    gather.loop(5 * span + LAG, gather.steps(), relaying)
    attend()
    gather.drain(GATE)

    def rs_copy(s, d, owner, dest):
        return pltpu.make_async_remote_copy(
            src_ref=part.at[s, pl.ds(pl.multiple_of(dest * rows, 16), rows)], dst_ref=rsbuf.at[s, owner],
            send_sem=rs_s.at[s, d - 1], recv_sem=rs_r.at[s, d - 1],
            device_id={"tp": lax.rem(tp + d, n_tp)}, device_id_type=MESH)

    def product(s):
        part[s] = (acc[s] + jnp.dot(delta_out[...], wbuf[OUT_DELTA, s], preferred_element_type=f32)).astype(bf16)
        for d in range(1, n_tp):
            rs_copy(s, d, tp, lax.rem(tp + d, n_tp)).start()

    def collect(s):
        total = part[s, pl.ds(pl.multiple_of(tp * rows, 16), rows)].astype(f32)
        for d in range(1, n_tp):
            owner = lax.rem(tp - d + n_tp, n_tp)
            rs_copy(s, d, owner, tp).wait_recv()
            total = total + rsbuf[s, owner].astype(f32)
        out_ref[:, pl.ds(pl.multiple_of(s * cols, cols), cols)] = total.astype(bf16)

    gather.finish(OUT_POOL)

    def pool_product(s):
        acc[s] = jnp.dot(pool_out[...], wbuf[OUT_POOL, s], preferred_element_type=f32)
    gather.loop(0, n_sp, pool_product)
    product(sp)
    advance(gather.steps(), gather.end())

    def arrive(t):
        gather.ready(OUT_DELTA, t)
        gather.each(t, lambda src, way: product(src))
    gather.loop(1, n_sp, arrive)
    gather.drain(OUT_POOL)

    @pl.when(sp < n_sp - 1)
    def _():
        for h in range(heads):
            state_copy(h).wait_send()
    collect(sp)
    gather.loop(1, n_sp, lambda t: gather.each(t, lambda src, way: collect(src)))
    gather.drain(OUT_DELTA)

    def sent(s):
        for d in range(1, n_tp):
            rs_copy(s, d, tp, lax.rem(tp + d, n_tp)).wait_send()
    gather.loop(0, n_sp, sent)


def per_device(
    tokens,
    norm_gain,
    w_pool_in,
    w_query,
    w_key,
    w_value,
    w_gate,
    w_beta,
    w_decay,
    conv_weight,
    a_log,
    decay_extra,
    w_mix,
    pool_scale,
    delta_gain,
    w_out_pool,
    w_out_delta,
):
    n_sp, n_fs, n_tp = (lax.axis_size(a) for a in ("sp", "fs", "tp"))
    weights = (w_key, w_query, w_value, w_pool_in, w_gate, w_out_pool, w_out_delta)
    rows, width = tokens.shape
    depth, cols = w_key.shape
    heads = a_log.shape[0]
    head_dim = cols // heads
    length = n_tp * rows
    unit = min(PAIR, length)
    count = len(weights)
    lanes = 128
    lane = lax.axis_index("tp")

    def own(w):
        return lax.dynamic_slice_in_dim(w, lane * heads, heads, 1)

    def wide(x):
        return jnp.pad(x, ((0, 0), (0, lanes - x.shape[1])))

    w_bd = wide(jnp.concatenate([own(w_decay), own(w_beta)], axis=1))
    slots = max(1, 2 ** max(0, len(share_bits(n_fs)) - 1) - 1)
    side = max(1, n_tp - 1)
    dma = pltpu.SemaphoreType.DMA
    vmem, anywhere = pl.BlockSpec(memory_space=pltpu.VMEM), pl.BlockSpec(memory_space=pl.ANY)
    return pl.pallas_call(
        functools.partial(mixer_kernel, n_sp, n_fs, n_tp),
        out_shape=jax.ShapeDtypeStruct((rows, width), bf16),
        in_specs=[anywhere] + [vmem] * 8 + [anywhere] * count,
        out_specs=vmem,
        scratch_shapes=[
            pltpu.VMEM((halo + length, width), bf16),
            pltpu.VMEM((halo + length, width), bf16),
            pltpu.VMEM((count, n_sp, depth, cols), bf16),
            pltpu.VMEM((5, halo + length, cols), f32),
            pltpu.VMEM((length, cols), bf16),
            pltpu.VMEM((length, cols), bf16),
            pltpu.VMEM((heads, length, 2 * head_dim), f32),
            pltpu.VMEM((heads, head_dim, 2 * head_dim), f32),
            pltpu.VMEM((heads, head_dim, head_dim), bf16),
            pltpu.VMEM((heads, head_dim, head_dim), bf16),
            pltpu.VMEM((n_sp, length, cols), bf16),
            pltpu.VMEM((n_sp, n_tp, rows, cols), bf16),
            pltpu.VMEM((heads, length, head_dim), f32),
            pltpu.VMEM((heads, length // unit, unit, unit), f32),
            pltpu.VMEM((heads, length, head_dim), f32),
            pltpu.VMEM((heads, length, head_dim), f32),
            pltpu.VMEM((heads, length, head_dim), f32),
            pltpu.VMEM((heads, length // unit, unit, unit), f32),
            pltpu.VMEM((2, length, lanes), f32),
            pltpu.VMEM((n_sp, length, cols), f32),
            dma((count + 1,)), dma((side,)), dma((side,)), dma((n_tp,)), dma((n_tp,)),
            dma((count, 2)), dma((count,)), dma((count, n_sp)), dma((count,)), dma((count, n_sp, slots)),
            dma((count, n_sp)), dma((heads,)), dma((heads,)), dma((n_sp, side)), dma((n_sp, side)),
        ],
        compiler_params=pltpu.CompilerParams(collective_id=0, has_side_effects=True, vmem_limit_bytes=56 << 20),
    )(tokens, norm_gain.reshape(1, -1), w_bd, conv_weight, wide(a_log.reshape(1, -1)), wide(decay_extra), w_mix,
      pool_scale.reshape(1, -1), delta_gain.reshape(1, -1), *weights)


def solution(mesh):
    placed = (
        P(("fs", "sp", "tp"), None),
        P(),
        P("sp", "tp"),
        P("sp", "tp"),
        P("sp", "tp"),
        P("sp", "tp"),
        P("sp", "tp"),
        P(),
        P(),
        P(None, None, "tp"),
        P("tp"),
        P(("fs", "sp"), "tp"),
        P("tp", None, None),
        P("tp"),
        P(),
        P("tp", "sp"),
        P("tp", "sp"),
    )
    return jax.shard_map(
        per_device,
        mesh=mesh,
        in_specs=placed,
        out_specs=P(("fs", "sp", "tp"), None),
        check_vma=False,
    )
```

time: 136 us -> 106 us (0.78)
  the two profiles are of different devices: /device:TPU:31 before, /device:TPU:0 now
where the time goes in v1:
time: 106 us
  Pallas kernels  98 us (92%)
  local copies, waits for them, and re-layouts  7.79 us (7%)
    pallas_call x1, Pallas kernels, per_device(): pl.pallas_call(functools.partial(mixer_kernel, n_sp, n_fs, n_tp), out_sha...  98 us
    pad x3, local copies, waits for them, and re-layouts, wide(): return jnp.pad(x, ((0, 0), (0, lanes - x.shape[1])))  2.78 us
    unnamed x6, local copies, waits for them, and re-layouts  2.67 us

profile of v1, /device:TPU:0, one launch (start us, length us, event | category | flops | bytes accessed | tf_op | source)
XLA Modules:
  0.0 105.8 jit_solution(7404988843786041988)
XLA Ops:
  0.0 0.0 copy-start
  0.0 1.2 %pad.13.refs_4_ = f32[1,128]{1,0:T(1,128)} pad(f32[1,4]{1,0:T(1,128)} %bitcast.5, f32[]{:T(128)} %constant.13.clone.1), padding=0_0x0_124 | pad | bytes 532 | tf_op jit(solution)/shard_map/jit(_pad)/pad | solution.py:607
  1.2 1.3 %reshape.12.refs_1_ = bf16[1,2048]{1,0:T(2,128)(2,1)} reshape(bf16[2048]{0:T(1024)(128)(2,1)} %param.18) | data formatting | bytes 8192 | tf_op jit(solution)/shard_map/reshape | solution.py:645
  2.5 0.0 copy-done
  2.5 0.8 constant_dynamic-slice_fusion
  3.3 0.0 copy-start.1
  3.3 0.6 copy-done.1
  4.0 0.1 copy.22
  4.1 0.7 pad.14.refs_5_
  4.8 0.3 copy.21
  5.1 0.9 pad.12.refs_2_
  6.0 98.0 %shard_map.163 = bf16[128,2048]{1,0:T(8,128)(2,1)} custom-call(bf16[128,2048]{1,0:T(8,128)(2,1)} %refs_0_.1, bf16[1,2048]{1,0:T(2,128)(2,1)} %reshape.12.refs_1_, bf16[2048,128]{1,0:T(8,128)(2,1)} %pad.12.refs_2_, f32[3,4,512]{2,1,0:T(4,128)} %refs_3_.1, f32[1,128]{1,0:T(1,128)} %pad.13.refs_4_, f32[256,128]{1,0:T(8,128)} %pad.14.refs_5_, ...), custom_call_target="tpu_custom_call" | custom-call | tf_op jit(solution)/shard_map/pallas_call | solution.py:614
  103.9 1.9 %copy.24 = bf16[128,2048]{1,0:T(8,128)(2,1)} copy(bf16[128,2048]{1,0:T(8,128)(2,1)} %shard_map.163) | data formatting | bytes 1048576
  (1 shorter events, 0.0 us)
Async XLA Ops:
  0.0 2.5 %copy-start = (bf16[2048,8]{0,1:T(8,128)(2,1)S(1)}, bf16[2048,8]{0,1:T(8,128)(2,1)}, u32[]{:S(2)}) copy-start(bf16[2048,8]{0,1:T(8,128)(2,1)} %param.24) | copy-start | bytes 98308
  3.3 0.7 copy-start.1

commit v2 on v1

--- a/solution.py
+++ b/solution.py
@@ -16,14 +16,27 @@
 highest = lax.Precision.HIGHEST
 f32 = jnp.float32
 bf16 = jnp.bfloat16
-KEY, QUERY, VALUE, POOL, GATE, OUT_POOL, OUT_DELTA = range(7)
+KEY, QUERY, VALUE, GATE, POOL, OUT_POOL, OUT_DELTA = range(7)
 AHEAD = 2
+SKEW = 2.0
+EARLY = 1.5
+FINAL = 1.1
 LAG = 2
 UNROLL = 32
 
 
 def mm(a, b, dims=((1,), (0,)), precision=highest):
     return lax.dot_general(a, b, (dims, ((), ())), precision=precision, preferred_element_type=f32)
+
+
+def halves(a):
+    high = a.astype(bf16)
+    return high, (a - high.astype(f32)).astype(bf16)
+
+
+def mm3(a, b, dims=((1,), (0,))):
+    (a_high, a_low), (b_high, b_low) = a, b
+    return (mm(a_high, b_high, dims, None) + mm(a_high, b_low, dims, None)) + mm(a_low, b_high, dims, None)
 
 
 def rms_rows(values, gain):
@@ -72,6 +85,7 @@
         self.pieces = 2 ** len(self.bits)
         self.mine = self.fs if self.bits else 0 * self.fs
         self.depth = wbuf.shape[2] // self.pieces
+        self.plan_order()
 
     def partner(self, bit):
         return self.fs + bit * (1 - 2 * (self.fs // bit % 2))
@@ -137,13 +151,50 @@
     def steps(self):
         return self.count * self.span
 
+    def plan_order(self):
+        span, count = self.span, self.count
+        if self.steps() > UNROLL:
+            self.order, self.sends = None, None
+            return
+        key = {(w, t): (max(0.0, w * span - (w > 0) * EARLY - (w == count - 1) * FINAL) + SKEW * (t - 1), w) for w in range(count) for t in range(1, span + 1)}
+        self.order = sorted(key, key=key.get)
+        self.sends = {}
+        for w in range(count):
+            i = self.order.index((w, 1)) if span else 0
+            while i > 0 and self.order[i - 1][1] == 1:
+                i -= 1
+            before = self.order[i - 1] if i > 0 else None
+            at = -1 if before is None or w < AHEAD else self.order.index((before[0], before[1] - 1))
+            self.sends.setdefault(at, []).append(w)
+
+    def place(self, w, t):
+        return self.order.index((w, t)) if self.order else w * self.span + t - 1
+
+    def pair(self, i):
+        if self.order:
+            return self.order[min(i, len(self.order) - 1)]
+        return i // self.span, i % self.span + 1
+
+    def early(self):
+        return self.sends.get(-1, []) if self.order else list(range(AHEAD))
+
     def step(self, i):
-        w, t = i // self.span, i % self.span + 1
+        if isinstance(i, int) and i < 0:
+            return
+        w, t = self.pair(i)
         when(i < self.steps(), lambda: self.each(t, lambda src, way: self.arrive_z(w, src, way)))
-        when(both(t == 1, w + AHEAD < self.count), lambda: self.send(w + AHEAD))
+        if self.order:
+            for later in self.sends.get(i, []):
+                self.send(later)
+        else:
+            when(both(t == 1, w + AHEAD < self.count), lambda: self.send(w + AHEAD))
         for k in range(len(self.bits) - 1):
             j = i - LAG * (k + 1)
-            when(both(j >= 0, j < self.steps()), lambda: self.arrive_f(j // self.span, j % self.span + 1, k))
+
+            def inner():
+                w, t = self.pair(j)
+                self.arrive_f(w, t, k)
+            when(both(j >= 0, j < self.steps()), inner)
 
     def end(self):
         return self.steps() + LAG * max(0, len(self.bits) - 1)
@@ -197,8 +248,10 @@
         greet({"fs": fs + bit * (1 - 2 * (fs // bit % 2))})
     for d in range(1, n_tp):
         greet({"tp": lax.rem(tp + d, n_tp)})
+    pl.when(both(left, tp < n_tp - 1))(lambda: greet({"sp": lax.rem(sp + n_sp - 1, n_sp), "tp": n_tp - 1}))
     heard = len(bits) + n_tp - 1
-    pl.semaphore_wait(barrier, heard + right.astype(jnp.int32) + left.astype(jnp.int32))
+    side = (n_tp - 1) * both(right, tp == n_tp - 1).astype(jnp.int32)
+    pl.semaphore_wait(barrier, heard + right.astype(jnp.int32) + left.astype(jnp.int32) + side)
 
 
 class Tokens:
@@ -214,17 +267,12 @@
             src_ref=ref, dst_ref=ref, send_sem=self.tok_s.at[d - 1], recv_sem=self.tok_r.at[d - 1],
             device_id={"tp": lax.rem(self.tp + d, self.n_tp)}, device_id_type=MESH)
 
-    def halo_next(self):
+    def halo_next(self, d):
         return pltpu.make_async_remote_copy(
             src_ref=self.tokbuf.at[pl.ds(self.n_tp * self.rows, halo)], dst_ref=self.tokbuf.at[pl.ds(0, halo)],
-            send_sem=self.halo_s.at[0], recv_sem=self.halo_r.at[0],
-            device_id={"sp": lax.rem(self.sp + 1, self.n_sp)}, device_id_type=MESH)
-
-    def halo_side(self, d):
-        ref = self.tokbuf.at[pl.ds(0, halo)]
-        return pltpu.make_async_remote_copy(
-            src_ref=ref, dst_ref=ref, send_sem=self.halo_s.at[d], recv_sem=self.halo_r.at[d],
-            device_id={"tp": lax.rem(self.tp + d, self.n_tp)}, device_id_type=MESH)
+            send_sem=self.halo_s.at[d], recv_sem=self.halo_r.at[0],
+            device_id={"sp": lax.rem(self.sp + 1, self.n_sp), "tp": lax.rem(self.tp + d, self.n_tp)},
+            device_id_type=MESH)
 
     def start(self):
         for d in range(1, self.n_tp):
@@ -233,29 +281,20 @@
     def start_halo(self):
         @pl.when(jnp.logical_and(self.tp == self.end, self.sp < self.n_sp - 1))
         def _():
-            self.halo_next().start()
+            for d in range(self.n_tp):
+                self.halo_next(d).start()
 
         @pl.when(self.sp == 0)
         def _():
             self.tokbuf[0:halo, :] = jnp.zeros((halo, self.tokbuf.shape[1]), self.tokbuf.dtype)
 
-    def relay(self):
-        @pl.when(jnp.logical_and(self.tp == self.end, self.sp > 0))
-        def _():
-            self.halo_next().wait_recv()
-            for d in range(1, self.n_tp):
-                self.halo_side(d).start()
-
     def finish(self):
         for d in range(1, self.n_tp):
             self.tok_copy(d, lax.rem(self.tp - d + self.n_tp, self.n_tp)).wait_recv()
 
-        @pl.when(jnp.logical_and(self.tp < self.end, self.sp > 0))
+        @pl.when(self.sp > 0)
         def _():
-            for d in range(1, self.n_tp):
-                @pl.when(self.tp == d - 1)
-                def _():
-                    self.halo_side(d).wait_recv()
+            self.halo_next(0).wait_recv()
 
     def drain(self):
         for d in range(1, self.n_tp):
@@ -263,21 +302,17 @@
 
         @pl.when(jnp.logical_and(self.tp == self.end, self.sp < self.n_sp - 1))
         def _():
-            self.halo_next().wait_send()
-
-        @pl.when(jnp.logical_and(self.tp == self.end, self.sp > 0))
-        def _():
-            for d in range(1, self.n_tp):
-                self.halo_side(d).wait_send()
+            for d in range(self.n_tp):
+                self.halo_next(d).wait_send()
 
 
 def mixer_kernel(n_sp, n_fs, n_tp, *refs):
-    tok_ref, gain_ref, wbd_ref, conv_ref, alog_ref, extra_ref, mix_ref, scale_ref, dgain_ref = refs[:9]
-    w_refs = refs[9:16]
-    out_ref = refs[16]
+    tok_ref, gain_ref, wb_ref, wd_ref, conv_ref, alog_ref, extra_ref, mix_ref, scale_ref, dgain_ref = refs[:10]
+    w_refs = refs[10:17]
+    out_ref = refs[17]
     (tokbuf, normbuf, wbuf, raw, pool_out, delta_out, pbuf, cbuf, s_in, s_out, part, rsbuf,
-     kbuf, xbuf, kwbuf, fbuf, qbuf, sbuf, gbuf, acc,
-     loc, tok_s, tok_r, halo_s, halo_r, z_s, z_f, z_r, f_s, f_r, last_r, st_s, st_r, rs_s, rs_r) = refs[17:]
+     kbuf, xbuf, ubuf, kwbuf, fbuf, qbuf, sbuf, gbuf, acc,
+     loc, tok_s, tok_r, halo_s, halo_r, z_s, z_f, z_r, f_s, f_r, last_r, st_s, st_r, rs_s, rs_r) = refs[18:]
     rows, width = tok_ref.shape
     length = n_tp * rows
     heads, head_dim = cbuf.shape[0], cbuf.shape[1]
@@ -303,14 +338,14 @@
     tokens.start()
     for w in range(1, count):
         local[w].wait()
-        if w < AHEAD:
+        if w in gather.early():
             gather.send(w)
     tokens.start_halo()
 
     def norm(a, b):
         def body(i, c):
             at = pl.ds(pl.multiple_of(i * 16, 16), 16)
-            normbuf[at, :] = rms_rows(tokbuf[at, :], gain_ref[...])
+            normbuf[at, :] = rms_rows(tokbuf[at, :], gain_ref[...].reshape(1, -1))
             return c
         lax.fori_loop(a, b, body, 0)
 
@@ -338,14 +373,30 @@
     strict = lower & (i2 > j2)
 
     def gates():
-        pre = jnp.dot(normbuf[...], wbd_ref[...], preferred_element_type=f32)[halo:]
+        lanes = gbuf.shape[2]
+        total = wb_ref.shape[0]
+        pick = jnp.where(
+            lax.broadcasted_iota(jnp.int32, (total, lanes), 0)
+            == tp * heads + lax.broadcasted_iota(jnp.int32, (total, lanes), 1), 1.0, 0.0)
+        lane = lax.broadcasted_iota(jnp.int32, (1, lanes), 1)
+        rate = jnp.zeros((1, lanes), f32)
+        for h in range(heads):
+            rate = jnp.where(lane == h, alog_ref[h], rate)
+        keep = jnp.where(
+            lax.broadcasted_iota(jnp.int32, (heads, lanes), 0)
+            == lax.broadcasted_iota(jnp.int32, (heads, lanes), 1), 1.0, 0.0)
+
+        def narrow(weight):
+            return mm(mm(normbuf[...], weight, ((1,), (1,)), None)[halo:], pick)
+        pre = narrow(wd_ref[...])
         softplus = jnp.maximum(pre, 0.0) + jnp.log1p(jnp.exp(-jnp.abs(pre)))
-        log_gate = -jnp.exp(alog_ref[...]) * softplus + extra_ref[...]
+        log_gate = -jnp.exp(rate) * softplus + mm(extra_ref[...], keep, ((0,), (0,)))
+        strength = narrow(wb_ref[...])
         row = lax.broadcasted_iota(jnp.int32, (length, length), 0)
         col = lax.broadcasted_iota(jnp.int32, (length, length), 1)
         tri = jnp.where((row // BLOCK == col // BLOCK) & (row >= col), 1.0, 0.0)
         cum = mm(tri, log_gate)
-        gbuf[0] = jax.nn.sigmoid(pre)
+        gbuf[0] = jax.nn.sigmoid(strength)
         gbuf[1] = cum
         cum_t = cum.T
         for p in range(per):
@@ -354,51 +405,56 @@
                 gaps = cum[at, h:h + 1] - cum_t[h:h + 1, at]
                 sbuf[h, p] = jnp.where(lower, jnp.exp(jnp.where(lower, gaps, 0.0)), 0.0)
 
+    all_units = [(h, p) for h in range(heads) for p in range(per)]
+
+    def rows_of(p):
+        return slice(p * unit, (p + 1) * unit)
+
     def keys(some):
         eye = jnp.where(i2 == j2, 1.0, 0.0)
-        units = []
         for h in some:
             k = unit_rows(active(1, KEY, h))
-            kb = k * gbuf[0, :, heads + h:heads + h + 1]
+            kb = k * gbuf[0, :, h:h + 1]
             kbuf[h] = k
             for p in range(per):
-                at = slice(p * unit, (p + 1) * unit)
-                corr = jnp.where(strict, mm(kb[at], k[at], ((1,), (1,))) * sbuf[h, p], 0.0)
-                units.append((h, p, corr))
+                at = rows_of(p)
+                corr = jnp.where(strict, mm3(halves(kb[at]), halves(k[at]), ((1,), (1,))) * sbuf[h, p], 0.0)
+                ubuf[h, p] = corr
+                xbuf[h, p] = eye - jnp.where(i2 // 2 == j2 // 2, corr, 0.0)
             kwbuf[h] = kb * jnp.exp(gbuf[1, :, h:h + 1])
-        done = [eye - jnp.where(i2 // 2 == j2 // 2, u[2], 0.0) for u in units]
-        size = 2
-        while size < BLOCK:
-            pair = (i2 // (2 * size) == j2 // (2 * size)) & (i2 // size != j2 // size)
-            half = [mm(jnp.where(pair, u[2], 0.0), x) for u, x in zip(units, done)]
-            done = [x - mm(x, y) for x, y in zip(done, half)]
-            size *= 2
-        for (h, p, _), x in zip(units, done):
-            at = slice(p * unit, (p + 1) * unit)
-            xbuf[h, p] = x
-            kwbuf[h, at] = mm(x, kwbuf[h, at])
+
+    def level(size):
+        pair = (i2 // (2 * size) == j2 // (2 * size)) & (i2 // size != j2 // size)
+        done = {u: halves(xbuf[u]) for u in all_units}
+        part_way = {u: mm3(halves(jnp.where(pair, ubuf[u], 0.0)), done[u]) for u in all_units}
+        for u in all_units:
+            xbuf[u] = xbuf[u] - mm3(done[u], halves(part_way[u]))
+
+    def key_weights():
+        for h, p in all_units:
+            kwbuf[h, rows_of(p)] = mm3(halves(xbuf[h, p]), halves(kwbuf[h, rows_of(p)]))
 
     def queries(some):
         for h in some:
             q = unit_rows(active(0, QUERY, h)) * head_dim ** (-0.5)
             qbuf[h] = q * jnp.exp(gbuf[1, :, h:h + 1])
             for p in range(per):
-                at = slice(p * unit, (p + 1) * unit)
-                sbuf[h, p] = mm(q[at], kbuf[h, at], ((1,), (1,))) * sbuf[h, p]
+                at = rows_of(p)
+                sbuf[h, p] = mm3(halves(q[at]), halves(kbuf[h, at]), ((1,), (1,))) * sbuf[h, p]
 
     def values(some):
         for h in some:
-            vb = active(2, VALUE, h) * gbuf[0, :, heads + h:heads + h + 1]
+            vb = active(2, VALUE, h) * gbuf[0, :, h:h + 1]
             for p in range(per):
-                at = slice(p * unit, (p + 1) * unit)
-                fbuf[h, at] = mm(xbuf[h, p], vb[at])
-
-    def scan():
+                at = rows_of(p)
+                fbuf[h, at] = mm3(halves(xbuf[h, p]), halves(vb[at]))
+
+    def scan(some):
         blank = jnp.concatenate([jnp.where(
             lax.broadcasted_iota(jnp.int32, (head_dim, head_dim), 0)
             == lax.broadcasted_iota(jnp.int32, (head_dim, head_dim), 1), 1.0, 0.0),
             jnp.zeros((head_dim, head_dim), f32)], axis=1)
-        for p in range(per):
+        for p in some:
             for b in range(unit // BLOCK):
                 at = slice(p * unit + b * BLOCK, p * unit + (b + 1) * BLOCK)
                 sub = slice(b * BLOCK, (b + 1) * BLOCK)
@@ -427,7 +483,7 @@
             tally = jnp.minimum(at_row + 1, span_of).astype(f32)
             pooled = (window[halo:] / tally - x[halo:]).astype(bf16)
             mixed = jnp.dot(pooled, mix_ref[i], preferred_element_type=f32)
-            pool_out[:, at] = (mixed * scale_ref[:, at]).astype(bf16)
+            pool_out[:, at] = (mixed * scale_ref[at].reshape(1, -1)).astype(bf16)
 
     def state_copy(h):
         return pltpu.make_async_remote_copy(
@@ -451,76 +507,7 @@
             at = slice(h * head_dim, (h + 1) * head_dim)
             attended = mm(pbuf[h, :, :head_dim], s_in[h].astype(f32), precision=None) + pbuf[h, :, head_dim:]
             scale = lax.rsqrt(jnp.mean(attended * attended, axis=-1, keepdims=True) + eps)
-            delta_out[:, at] = (attended * scale * dgain_ref[...] * silu(raw[GATE, halo:, at])).astype(bf16)
-
-    first = 4 * span
-
-    def turn(r):
-        return first + 7 * r // 3
-
-    def plain(i):
-        gather.step(i)
-
-    def relaying(i):
-        gather.step(i)
-        if isinstance(i, int):
-            for r in range(n_sp):
-                if turn(r) == i:
-                    pl.when(sp == r)(relay)
-        else:
-            pl.when(i == turn(sp))(relay)
-
-    def advance(a, b):
-        gather.loop(a, b, plain)
-
-    half = (heads + 1) // 2
-    low = halo // 16 + tp * (rows // 16)
-    high = low + rows // 16
-    first_part, second_part = range(half), range(half, heads)
-
-    @pl.when(sp == 0)
-    def _():
-        s_in[...] = jnp.zeros_like(s_in)
-    advance(0, 1)
-    norm(low, high)
-    advance(1, span)
-    tokens.relay()
-    advance(span, span + 1)
-    tokens.finish()
-    norm(0, low)
-    norm(high, tokbuf.shape[0] // 16)
-    gates()
-    at = span + LAG
-    advance(span + 1, at)
-    gather.finish(KEY)
-    project(KEY)
-    keys(first_part)
-    advance(at, at + 1)
-    keys(second_part)
-    advance(at + 1, 2 * span + LAG)
-    gather.finish(QUERY)
-    project(QUERY)
-    queries(range(heads))
-    gather.drain(KEY)
-    advance(2 * span + LAG, 3 * span + LAG)
-    gather.finish(VALUE)
-    project(VALUE)
-    values(range(heads))
-    gather.drain(QUERY)
-    scan()
-    gather.loop(3 * span + LAG, 4 * span + LAG, relaying)
-    gather.finish(POOL)
-    project(POOL)
-    pool()
-    gather.drain(VALUE)
-    gather.loop(4 * span + LAG, 5 * span + LAG, relaying)
-    gather.finish(GATE)
-    project(GATE)
-    gather.drain(POOL)
-    tokens.drain()
-    gather.loop(5 * span + LAG, gather.steps(), relaying)
-    attend()
-    gather.drain(GATE)
+            delta_out[:, at] = (attended * scale * dgain_ref[...].reshape(1, -1) * silu(raw[GATE, halo:, at])).astype(bf16)
 
     def rs_copy(s, d, owner, dest):
         return pltpu.make_async_remote_copy(
@@ -541,18 +528,77 @@
             total = total + rsbuf[s, owner].astype(f32)
         out_ref[:, pl.ds(pl.multiple_of(s * cols, cols), cols)] = total.astype(bf16)
 
-    gather.finish(OUT_POOL)
-
     def pool_product(s):
         acc[s] = jnp.dot(pool_out[...], wbuf[OUT_POOL, s], preferred_element_type=f32)
-    gather.loop(0, n_sp, pool_product)
-    product(sp)
-    advance(gather.steps(), gather.end())
+
+    def ready(w):
+        return max([gather.place(w, t) for t in range(1, n_sp)], default=0) + LAG
+
+    turns = ready(VALUE) + 2
+
+    def step(i):
+        gather.step(i)
+        if isinstance(i, int):
+            for r in range(n_sp):
+                if turns + 2 * r == i:
+                    pl.when(sp == r)(relay)
+        else:
+            pl.when(i == turns + 2 * sp)(relay)
+
+    half = (heads + 1) // 2
+    middle = (per + 1) // 2
+    low = halo // 16 + tp * (rows // 16)
+    high = low + rows // 16
+    left, right = range(half), range(half, heads)
+    sizes = [2 << i for i in range((BLOCK // 2).bit_length() - 1)]
+
+    @pl.when(sp == 0)
+    def _():
+        s_in[...] = jnp.zeros_like(s_in)
+
+    def arrive_pool(t):
+        gather.ready(OUT_POOL, t)
+        gather.each(t, lambda src, way: pool_product(src))
 
     def arrive(t):
         gather.ready(OUT_DELTA, t)
         gather.each(t, lambda src, way: product(src))
-    gather.loop(1, n_sp, arrive)
+
+    attend_at = max(turns + 2 * span, ready(POOL) + 2)
+    plan = [
+        (0, lambda: norm(low, high)),
+        (span - 1, tokens.finish), (span - 1, lambda: norm(0, low)),
+        (span, lambda: norm(high, tokbuf.shape[0] // 16)), (span, gates),
+        (ready(KEY), lambda: gather.finish(KEY)), (ready(KEY), lambda: project(KEY)),
+        (ready(KEY) + 1, lambda: keys(left)), (ready(KEY) + 1, lambda: keys(right)),
+        (ready(QUERY), lambda: gather.finish(QUERY)), (ready(QUERY), lambda: project(QUERY)),
+        (ready(QUERY) + 2, key_weights), (ready(QUERY) + 2, lambda: queries(left)),
+        (ready(QUERY) + 2, lambda: gather.drain(KEY)), (ready(QUERY) + 2, lambda: queries(right)),
+        (ready(VALUE), lambda: gather.finish(VALUE)), (ready(VALUE), lambda: project(VALUE)),
+        (ready(VALUE), lambda: values(range(heads))), (ready(VALUE), lambda: scan(range(middle))),
+        (ready(VALUE) + 1, lambda: scan(range(middle, per))), (ready(VALUE) + 1, lambda: gather.drain(QUERY)),
+        (ready(GATE) + 1, lambda: gather.finish(GATE)), (ready(GATE) + 1, lambda: project(GATE)),
+        (ready(GATE) + 1, lambda: gather.drain(VALUE)), (ready(GATE) + 1, tokens.drain),
+        (ready(POOL), lambda: gather.finish(POOL)), (ready(POOL), lambda: project(POOL)),
+        (ready(POOL) + 1, pool), (ready(POOL) + 1, lambda: gather.drain(GATE)),
+        (ready(POOL) + 2, lambda: pool_product(sp)),
+        (attend_at, attend), (attend_at, lambda: product(sp)), (attend_at, lambda: gather.drain(POOL)),
+        (gather.end() - 1, lambda: None),
+    ]
+    where = [ready(KEY) + 2, ready(KEY) + 2, ready(QUERY), ready(QUERY) + 1, ready(QUERY) + 1]
+    for n, size in enumerate(sizes):
+        plan.append((where[min(n, len(where) - 1)], functools.partial(level, size)))
+    for t in range(1, n_sp):
+        pooled_at = gather.place(OUT_POOL, t) + LAG
+        plan.append((max(ready(POOL) + 2, pooled_at), functools.partial(arrive_pool, t)))
+        plan.append((max(attend_at, pooled_at, gather.place(OUT_DELTA, t) + LAG), functools.partial(arrive, t)))
+    plan.sort(key=lambda entry: entry[0])
+    reached = 0
+    for at_step, act in plan:
+        if at_step >= reached:
+            gather.loop(reached, at_step + 1, step)
+            reached = at_step + 1
+        act()
     gather.drain(OUT_POOL)
 
     @pl.when(sp < n_sp - 1)
@@ -589,7 +635,7 @@
     w_out_delta,
 ):
     n_sp, n_fs, n_tp = (lax.axis_size(a) for a in ("sp", "fs", "tp"))
-    weights = (w_key, w_query, w_value, w_pool_in, w_gate, w_out_pool, w_out_delta)
+    weights = (w_key, w_query, w_value, w_gate, w_pool_in, w_out_pool, w_out_delta)
     rows, width = tokens.shape
     depth, cols = w_key.shape
     heads = a_log.shape[0]
@@ -598,23 +644,15 @@
     unit = min(PAIR, length)
     count = len(weights)
     lanes = 128
-    lane = lax.axis_index("tp")
-
-    def own(w):
-        return lax.dynamic_slice_in_dim(w, lane * heads, heads, 1)
-
-    def wide(x):
-        return jnp.pad(x, ((0, 0), (0, lanes - x.shape[1])))
-
-    w_bd = wide(jnp.concatenate([own(w_decay), own(w_beta)], axis=1))
     slots = max(1, 2 ** max(0, len(share_bits(n_fs)) - 1) - 1)
     side = max(1, n_tp - 1)
     dma = pltpu.SemaphoreType.DMA
     vmem, anywhere = pl.BlockSpec(memory_space=pltpu.VMEM), pl.BlockSpec(memory_space=pl.ANY)
+    scalars = pl.BlockSpec(memory_space=pltpu.SMEM)
     return pl.pallas_call(
         functools.partial(mixer_kernel, n_sp, n_fs, n_tp),
         out_shape=jax.ShapeDtypeStruct((rows, width), bf16),
-        in_specs=[anywhere] + [vmem] * 8 + [anywhere] * count,
+        in_specs=[anywhere] + [vmem] * 4 + [scalars] + [vmem] * 4 + [anywhere] * count,
         out_specs=vmem,
         scratch_shapes=[
             pltpu.VMEM((halo + length, width), bf16),
@@ -631,19 +669,19 @@
             pltpu.VMEM((n_sp, n_tp, rows, cols), bf16),
             pltpu.VMEM((heads, length, head_dim), f32),
             pltpu.VMEM((heads, length // unit, unit, unit), f32),
+            pltpu.VMEM((heads, length // unit, unit, unit), f32),
             pltpu.VMEM((heads, length, head_dim), f32),
             pltpu.VMEM((heads, length, head_dim), f32),
             pltpu.VMEM((heads, length, head_dim), f32),
             pltpu.VMEM((heads, length // unit, unit, unit), f32),
             pltpu.VMEM((2, length, lanes), f32),
             pltpu.VMEM((n_sp, length, cols), f32),
-            dma((count + 1,)), dma((side,)), dma((side,)), dma((n_tp,)), dma((n_tp,)),
+            dma((count + 1,)), dma((side,)), dma((side,)), dma((n_tp,)), dma((1,)),
             dma((count, 2)), dma((count,)), dma((count, n_sp)), dma((count,)), dma((count, n_sp, slots)),
             dma((count, n_sp)), dma((heads,)), dma((heads,)), dma((n_sp, side)), dma((n_sp, side)),
         ],
         compiler_params=pltpu.CompilerParams(collective_id=0, has_side_effects=True, vmem_limit_bytes=56 << 20),
-    )(tokens, norm_gain.reshape(1, -1), w_bd, conv_weight, wide(a_log.reshape(1, -1)), wide(decay_extra), w_mix,
-      pool_scale.reshape(1, -1), delta_gain.reshape(1, -1), *weights)
+    )(tokens, norm_gain, w_beta.T, w_decay.T, conv_weight, a_log, decay_extra.T, w_mix, pool_scale, delta_gain, *weights)
 
 
 def solution(mesh):

time: 106 us -> 83.4 us (0.79)
  Pallas kernels: 98 us -> 81.4 us
  local copies, waits for them, and re-layouts: 7.79 us -> 1.88 us
    pallas_call x1, Pallas kernels: 98 us -> 81.4 us  [per_device(): pl.pallas_call(functools.partial(mixer_kernel, n_sp, n_fs, n_tp), out_sha...]
    pad x3 -> x0, local copies, waits for them, and re-layouts: 2.78 us -> none  [wide(): return jnp.pad(x, ((0, 0), (0, lanes - x.shape[1])))]
    reshape x1 -> x0, local copies, waits for them, and re-layouts: 1.3 us -> none  [per_device(): norm_gain.reshape(1, -1)]
    unnamed x6 -> x1, local copies, waits for them, and re-layouts: 2.67 us -> 1.88 us
where the time goes in v2:
time: 83.4 us; the launch traced here: 83.2 us
  Pallas kernels  81.4 us (98%)
  local copies, waits for them, and re-layouts  1.88 us (2%)
    pallas_call x1, Pallas kernels, per_device(): pl.pallas_call(functools.partial(mixer_kernel, n_sp, n_fs, n_tp), out_sha...  81.4 us
    unnamed x1, local copies, waits for them, and re-layouts  1.88 us

profile of v2, /device:TPU:0, one launch (start us, length us, event | category | flops | bytes accessed | tf_op | source)
XLA Modules:
  0.0 83.2 jit_solution(12978182928009670436)
XLA Ops:
  0.0 81.4 %shard_map.163 = bf16[128,2048]{1,0:T(8,128)(2,1)} custom-call(bf16[128,2048]{1,0:T(8,128)(2,1)} %refs_0_.1, bf16[2048]{0:T(1024)(128)(2,1)} %refs_1_.1, bf16[8,2048]{1,0:T(8,128)(2,1)} %bitcast.3, bf16[8,2048]{1,0:T(8,128)(2,1)} %bitcast.4, f32[3,4,512]{2,1,0:T(4,128)} %refs_4_.1, f32[4]{0:T(128)} %refs_5_.1, f32[4,256]{1,0:T(4,128)} %bitcast.5, ...), custom_call_target="tpu_custom_call" | custom-call | tf_op jit(solution)/shard_map/pallas_call | solution.py:652
  81.4 1.9 %copy.19 = bf16[128,2048]{1,0:T(8,128)(2,1)} copy(bf16[128,2048]{1,0:T(8,128)(2,1)} %shard_map.163) | data formatting | bytes 1048576

commit v3 on v2

--- a/solution.py
+++ b/solution.py
@@ -649,9 +649,9 @@
     dma = pltpu.SemaphoreType.DMA
     vmem, anywhere = pl.BlockSpec(memory_space=pltpu.VMEM), pl.BlockSpec(memory_space=pl.ANY)
     scalars = pl.BlockSpec(memory_space=pltpu.SMEM)
-    return pl.pallas_call(
+    mixed = pl.pallas_call(
         functools.partial(mixer_kernel, n_sp, n_fs, n_tp),
-        out_shape=jax.ShapeDtypeStruct((rows, width), bf16),
+        out_shape=pltpu.VMEM((rows, width), bf16),
         in_specs=[anywhere] + [vmem] * 4 + [scalars] + [vmem] * 4 + [anywhere] * count,
         out_specs=vmem,
         scratch_shapes=[
@@ -683,6 +683,8 @@
         compiler_params=pltpu.CompilerParams(collective_id=0, has_side_effects=True, vmem_limit_bytes=56 << 20),
     )(tokens, norm_gain, w_beta.T, w_decay.T, conv_weight, a_log, decay_extra.T, w_mix, pool_scale, delta_gain, *weights)
 
+    return mixed
+
 
 def solution(mesh):
     placed = (

time: 83.4 us -> 81.5 us (0.977)
  local copies, waits for them, and re-layouts: 1.88 us -> 0.8 us
    unnamed x1, local copies, waits for them, and re-layouts: 1.88 us -> 0.8 us
where the time goes in v3:
time: 81.5 us; the launch traced here: 81.4 us
  Pallas kernels  80.6 us (99%)
    pallas_call x1, Pallas kernels, per_device(): pl.pallas_call(functools.partial(mixer_kernel, n_sp, n_fs, n_tp), out_sha...  80.6 us

profile of v3, /device:TPU:0, one launch (start us, length us, event | category | flops | bytes accessed | tf_op | source)
XLA Modules:
  0.0 81.4 jit_solution(3272300767140177987)
XLA Ops:
  0.0 80.6 %shard_map.163 = bf16[128,2048]{1,0:T(8,128)(2,1)S(1)} custom-call(bf16[128,2048]{1,0:T(8,128)(2,1)} %refs_0_.1, bf16[2048]{0:T(1024)(128)(2,1)} %refs_1_.1, bf16[8,2048]{1,0:T(8,128)(2,1)} %bitcast.3, bf16[8,2048]{1,0:T(8,128)(2,1)} %bitcast.4, f32[3,4,512]{2,1,0:T(4,128)} %refs_4_.1, f32[4]{0:T(128)} %refs_5_.1, f32[4,256]{1,0:T(4,128)} %bitcast.5, ...), custom_call_target="tpu_custom_call" | custom-call | tf_op jit(solution)/shard_map/pallas_call | solution.py:652
  80.6 0.8 copy.19

commit v4 on v3

--- a/solution.py
+++ b/solution.py
@@ -307,12 +307,15 @@
 
 
 def mixer_kernel(n_sp, n_fs, n_tp, *refs):
-    tok_ref, gain_ref, wb_ref, wd_ref, conv_ref, alog_ref, extra_ref, mix_ref, scale_ref, dgain_ref = refs[:10]
+    tok_ref, given = refs[0], refs[1:10]
     w_refs = refs[10:17]
     out_ref = refs[17]
     (tokbuf, normbuf, wbuf, raw, pool_out, delta_out, pbuf, cbuf, s_in, s_out, part, rsbuf,
      kbuf, xbuf, ubuf, kwbuf, fbuf, qbuf, sbuf, gbuf, acc,
-     loc, tok_s, tok_r, halo_s, halo_r, z_s, z_f, z_r, f_s, f_r, last_r, st_s, st_r, rs_s, rs_r) = refs[18:]
+     loc, tok_s, tok_r, halo_s, halo_r, z_s, z_f, z_r, f_s, f_r, last_r, st_s, st_r, rs_s, rs_r, small_s) = refs[18:-9]
+    held = refs[-9:]
+    gain_ref, wb_ref, wd_ref, conv_ref, alog_ref, extra_ref, mix_ref, scale_ref, dgain_ref = held
+    small = [pltpu.make_async_copy(a, b, small_s.at[i]) for i, (a, b) in enumerate(zip(given, held))]
     rows, width = tok_ref.shape
     length = n_tp * rows
     heads, head_dim = cbuf.shape[0], cbuf.shape[1]
@@ -326,7 +329,7 @@
         tok_ref, tokbuf.at[pl.ds(pl.multiple_of(halo + tp * rows, 16), rows)], loc.at[count])
     local[0].start()
     here.start()
-    for copy in local[1:]:
+    for copy in local[1:] + small:
         copy.start()
     enter(n_sp, n_fs, n_tp)
     tokens = Tokens(n_sp, n_tp, tokbuf, rows, tok_s, tok_r, halo_s, halo_r)
@@ -341,6 +344,8 @@
         if w in gather.early():
             gather.send(w)
     tokens.start_halo()
+    for copy in small:
+        copy.wait()
 
     def norm(a, b):
         def body(i, c):
@@ -648,11 +653,12 @@
     side = max(1, n_tp - 1)
     dma = pltpu.SemaphoreType.DMA
     vmem, anywhere = pl.BlockSpec(memory_space=pltpu.VMEM), pl.BlockSpec(memory_space=pl.ANY)
-    scalars = pl.BlockSpec(memory_space=pltpu.SMEM)
+    small = (norm_gain, w_beta.T, w_decay.T, conv_weight, a_log, decay_extra.T, w_mix, pool_scale, delta_gain)
+    held = [(pltpu.SMEM if a is a_log else pltpu.VMEM)(a.shape, a.dtype) for a in small]
     mixed = pl.pallas_call(
         functools.partial(mixer_kernel, n_sp, n_fs, n_tp),
         out_shape=pltpu.VMEM((rows, width), bf16),
-        in_specs=[anywhere] + [vmem] * 4 + [scalars] + [vmem] * 4 + [anywhere] * count,
+        in_specs=[anywhere] * (10 + count),
         out_specs=vmem,
         scratch_shapes=[
             pltpu.VMEM((halo + length, width), bf16),
@@ -679,9 +685,10 @@
             dma((count + 1,)), dma((side,)), dma((side,)), dma((n_tp,)), dma((1,)),
             dma((count, 2)), dma((count,)), dma((count, n_sp)), dma((count,)), dma((count, n_sp, slots)),
             dma((count, n_sp)), dma((heads,)), dma((heads,)), dma((n_sp, side)), dma((n_sp, side)),
+            dma((9,)), *held,
         ],
         compiler_params=pltpu.CompilerParams(collective_id=0, has_side_effects=True, vmem_limit_bytes=56 << 20),
-    )(tokens, norm_gain, w_beta.T, w_decay.T, conv_weight, a_log, decay_extra.T, w_mix, pool_scale, delta_gain, *weights)
+    )(tokens, *small, *weights)
 
     return mixed
 

time: 81.5 us -> 80.6 us (0.989)
  Pallas kernels: 80.6 us -> 79.6 us
    pallas_call x1, Pallas kernels: 80.6 us -> 79.6 us  [per_device(): pl.pallas_call(functools.partial(mixer_kernel, n_sp, n_fs, n_tp), out_sha...]
where the time goes in v4:
time: 80.6 us; the launch traced here: 80.4 us
  Pallas kernels  79.6 us (99%)
    pallas_call x1, Pallas kernels, per_device(): pl.pallas_call(functools.partial(mixer_kernel, n_sp, n_fs, n_tp), out_sha...  79.6 us

profile of v4, /device:TPU:0, one launch (start us, length us, event | category | flops | bytes accessed | tf_op | source)
XLA Modules:
  0.0 80.4 jit_solution(5320445154619455223)
XLA Ops:
  0.0 79.6 %shard_map.163 = bf16[128,2048]{1,0:T(8,128)(2,1)S(1)} custom-call(bf16[128,2048]{1,0:T(8,128)(2,1)} %refs_0_.1, bf16[2048]{0:T(1024)(128)(2,1)} %refs_1_.1, bf16[8,2048]{1,0:T(8,128)(2,1)} %bitcast.3, bf16[8,2048]{1,0:T(8,128)(2,1)} %bitcast.4, f32[3,4,512]{2,1,0:T(4,128)} %refs_4_.1, f32[4]{0:T(128)} %refs_5_.1, f32[4,256]{1,0:T(4,128)} %bitcast.5, ...), custom_call_target="tpu_custom_call" | custom-call | tf_op jit(solution)/shard_map/pallas_call | solution.py:658
  79.7 0.8 copy.19
